TPU v7x, 32 devices: a whole 2x2x4 slice. The times are simulated.
32 devices in a mesh: sp: 8 (over z, x), tp: 4 (over y, core).
Axes of the slice: x: 2, y: 2, z: 4, core: 2. Of those that a mesh axis runs over, the one named last changes fastest.
Arguments:
- queries: bfloat16 [4096, 1024], P('sp', 'tp'), may hold values from -100 to 100
- keys: bfloat16 [4096, 256], P('sp', 'tp'), may hold values from -100 to 100
- values: bfloat16 [4096, 256], P('sp', 'tp'), may hold values from -6 to 6
- sink_logits: float32 [16], P('tp'), may hold values from 2 to 6
- stream: bfloat16 [4096, 2048], P(('sp', 'tp')), may hold values from -6 to 6
- out_proj: bfloat16 [1024, 2048], P('tp'), may hold values from -0.1875 to 0.1875
- norm_gain: float32 [2048], replicated, may hold values from 0.1 to 1.9
- routes: int32 [4096, 2], P(('sp', 'tp')), may hold values from 0 to 7, all different within a row; in each aligned block of 128 rows (0 to 127, 128 to 255, ...) at most 40 rows name the same one
- route_weights: float32 [4096, 2], P(('sp', 'tp')), may hold values from 0.2 to 1
- gate_proj: bfloat16 [8, 2048, 3584], P('sp', None, 'tp'), may hold values from -0.125 to 0.125
- up_proj: bfloat16 [8, 2048, 3584], P('sp', None, 'tp'), may hold values from -0.125 to 0.125
- down_proj: bfloat16 [8, 3584, 2048], P('sp', 'tp'), may hold values from -0.09375 to 0.09375
Outputs:
- layer_out: bfloat16 [4096, 2048], P(('sp', 'tp'))
Inputs may be any that keep to these rules, and one draw needn't show every extreme that they name: `routes`: each row names two different experts. Among the rows of one device after the attention (aligned blocks of 128 rows) no expert is named more than 40 times.
All inputs are finite; a program needn't handle non-finite values.
Results may differ from a plain program's by a relative error of at most 0.009.
Values may be sent and summed in bfloat16 or wider, within the bound.
A program may use at most 128 MiB of HBM per device.

v0:
```python
import jax
import jax.numpy as jnp
from jax import lax
from jax.sharding import PartitionSpec as P

DH = 64
WINDOW = 128


EPSILON = 1e-06


def from_behind(value, axis, by):
    length = lax.axis_size(axis)
    pairs = [(i, i + by) for i in range(length) if 0 <= i + by < length]
    return lax.ppermute(value, axis, pairs)


def attend(queries, keys, values, sink_logits):
    tok_sp = queries.shape[0]
    heads_here = sink_logits.shape[0]
    kv_here = keys.shape[1] // DH
    group = heads_here // kv_here
    tail_rows = from_behind((keys[tok_sp - WINDOW :], values[tok_sp - WINDOW :]), "sp", 1)
    blocks = tok_sp // WINDOW
    key_all = jnp.concatenate([tail_rows[0], keys], axis=0).reshape(blocks + 1, WINDOW, kv_here, DH)
    value_all = jnp.concatenate([tail_rows[1], values], axis=0).reshape(
        blocks + 1, WINDOW, kv_here, DH
    )
    key_band = jnp.concatenate([key_all[:-1], key_all[1:]], axis=1)
    value_band = jnp.concatenate([value_all[:-1], value_all[1:]], axis=1)
    query_blocks = queries.reshape(blocks, WINDOW, kv_here, group, DH)
    scores = jnp.einsum(
        "nqkgd,nskd->nkgqs", query_blocks, key_band, preferred_element_type=jnp.float32
    ) * DH ** (-0.5)
    offset = lax.axis_index("sp") * tok_sp
    query_pos = jnp.arange(WINDOW, dtype=jnp.int32)[:, None] + WINDOW
    key_pos = jnp.arange(2 * WINDOW, dtype=jnp.int32)[None, :]
    distance = query_pos - key_pos
    block_first = offset + jnp.arange(blocks, dtype=jnp.int32) * WINDOW - WINDOW
    key_abs = block_first[:, None] + jnp.arange(2 * WINDOW, dtype=jnp.int32)[None, :]
    allowed = ((distance >= 0) & (distance < WINDOW))[None] & (key_abs >= 0)[:, None, :]
    logits = jnp.where(allowed[:, None, None], scores, -jnp.inf)
    sink_part = sink_logits.reshape(kv_here, group)[None, :, :, None]
    highest = jnp.maximum(jnp.max(logits, axis=-1), sink_part)
    expo = jnp.exp(logits - highest[..., None])
    denominator = jnp.sum(expo, axis=-1) + jnp.exp(sink_part - highest)
    weights = (expo / denominator[..., None]).astype(jnp.bfloat16)
    mixed_heads = jnp.einsum(
        "nkgqs,nskd->nqkgd", weights, value_band, preferred_element_type=jnp.float32
    )
    return mixed_heads.reshape(tok_sp, heads_here * DH).astype(jnp.bfloat16)


def build_send(block_rows, block_routes, experts, capacity):
    tokens_here = block_rows.shape[0]
    flat_ids = block_routes.reshape(-1)
    hits = (flat_ids[:, None] == jnp.arange(experts, dtype=jnp.int32)[None, :]).astype(jnp.int32)
    earlier = jnp.sum((jnp.cumsum(hits, axis=0) - hits) * hits, axis=1)
    slot_ids = flat_ids * capacity + earlier
    slot_total = experts * capacity
    chosen = slot_ids[None, :] == jnp.arange(slot_total, dtype=jnp.int32)[:, None]
    picker = jnp.any(chosen.reshape(slot_total, tokens_here, block_routes.shape[1]), axis=2).astype(
        jnp.bfloat16
    )
    outgoing = jnp.dot(picker, block_rows, preferred_element_type=jnp.float32).astype(jnp.bfloat16)
    return (outgoing, slot_ids.reshape(tokens_here, block_routes.shape[1]))


def on_device(
    queries,
    keys,
    values,
    sink_logits,
    stream,
    out_proj,
    norm_gain,
    routes,
    route_weights,
    gate_proj,
    up_proj,
    down_proj,
):
    attended = attend(queries, keys, values, sink_logits)
    tok_dev = stream.shape[0]
    regrouped = lax.all_to_all(attended, "tp", split_axis=0, concat_axis=1, tiled=True)
    projected = jnp.dot(
        regrouped,
        lax.all_gather(out_proj, "tp", axis=0, tiled=True),
        preferred_element_type=jnp.float32,
    )
    mixed = stream.astype(jnp.float32) + projected
    scale = lax.rsqrt(jnp.mean(mixed * mixed, axis=-1, keepdims=True) + EPSILON)
    normed = (mixed * scale * norm_gain).astype(jnp.bfloat16)
    experts = lax.axis_size("sp")
    capacity = max(2, (5 * tok_dev + 2 * experts - 1) // (2 * experts))
    outgoing, slot_ids = build_send(normed, routes, experts, capacity)
    arrived = lax.all_to_all(outgoing, "sp", split_axis=0, concat_axis=0, tiled=True)
    expert_input = lax.all_gather(arrived, "tp", axis=0, tiled=True)
    gate_part = jnp.dot(expert_input, gate_proj[0], preferred_element_type=jnp.float32)
    up_part = jnp.dot(expert_input, up_proj[0], preferred_element_type=jnp.float32)
    hidden = (jax.nn.silu(gate_part) * up_part).astype(jnp.bfloat16)
    partial_value = jnp.dot(hidden, down_proj[0], preferred_element_type=jnp.float32)
    summed = lax.psum_scatter(
        partial_value.astype(jnp.bfloat16), "tp", scatter_dimension=0, tiled=True
    )
    returned = lax.all_to_all(summed, "sp", split_axis=0, concat_axis=0, tiled=True)
    first_out = jnp.take(returned, slot_ids[:, 0], axis=0).astype(jnp.float32)
    second_out = jnp.take(returned, slot_ids[:, 1], axis=0).astype(jnp.float32)
    result = mixed + route_weights[:, 0:1] * first_out + route_weights[:, 1:2] * second_out
    return result.astype(jnp.bfloat16)


def solution(mesh):
    return jax.shard_map(
        on_device,
        mesh=mesh,
        in_specs=(
            P("sp", "tp"),
            P("sp", "tp"),
            P("sp", "tp"),
            P("tp"),
            P(("sp", "tp"), None),
            P("tp", None),
            P(),
            P(("sp", "tp"), None),
            P(("sp", "tp"), None),
            P("sp", None, "tp"),
            P("sp", None, "tp"),
            P("sp", "tp", None),
        ),
        out_specs=P(("sp", "tp"), None),
        check_vma=False,
    )
```

profile of v0, /device:TPU:0, one launch (start us, length us, event | category | flops | bytes accessed | tf_op | source)
XLA Modules:
  0.0 253.8 jit_solution(625209890800368560)
XLA Ops:
  6.5 0.0 copy-start.3
  6.5 0.0 all-gather.3.cloned.1.call-start
  6.5 0.7 all-gather.3.cloned.1.call-update
  7.3 0.7 slice.48
  8.0 4.9 %collective-permute-start.1 = (bf16[128,64]{0,1:T(8,128)(2,1)S(1)}, bf16[128,64]{0,1:T(8,128)(2,1)S(1)}, u32[]{:S(2)}, u32[]{:S(2)}) collective-permute-start(bf16[128,64]{0,1:T(8,128)(2,1)S(1)} %slice.48), channel_id=1, source_target_pairs={{0,4},{4,8},{8,12},{12,16},{16,20},{20,24},{24,28},{1,5},{5,9},{9,... | collective-permute-start | bytes 49160 | tf_op jit(solution)/shard_map/ppermute | solution.py:16
  12.8 0.7 slice.44
  13.6 3.4 %collective-permute-start = (bf16[128,64]{0,1:T(8,128)(2,1)S(1)}, bf16[128,64]{0,1:T(8,128)(2,1)S(1)}, u32[]{:S(2)}, u32[]{:S(2)}) collective-permute-start(bf16[128,64]{0,1:T(8,128)(2,1)S(1)} %slice.44), channel_id=1, source_target_pairs={{0,4},{4,8},{8,12},{12,16},{16,20},{20,24},{24,28},{1,5},{5,9},{9,... | collective-permute-start | bytes 49160 | tf_op jit(solution)/shard_map/ppermute | solution.py:16
  17.0 0.8 copy.57
  17.8 0.1 eq.43
  18.0 0.1 eq.39
  18.1 0.6 reduce-window.6
  18.7 0.2 slice_reduce_fusion
  19.0 0.1 add_compare_fusion
  19.1 0.2 broadcast_and_fusion
  19.3 0.1 fusion.18
  19.4 0.9 slice.51
  20.3 0.9 slice.47
  21.1 1.3 reshape.197
  22.4 0.1 reduce_sum.31
  22.6 0.1 copy.59
  22.6 0.0 collective-permute-done.1
  22.6 0.8 pad_maximum_fusion
  23.5 0.0 collective-permute-done
  23.5 0.8 pad_maximum_fusion.1
  24.4 0.5 fusion.22
  24.9 0.0 copy-done.3
  24.9 0.1 broadcast_maximum_fusion
  25.0 0.3 fusion.4
  25.3 0.1 exponential_add_fusion
  25.4 0.0 copy-start.2
  25.4 0.0 copy-start
  25.4 1.2 convolution_convert_fusion.2
  26.6 0.0 copy-start.1
  26.6 3.5 %all-to-all-start = ((bf16[4,128,256]{1,2,0:T(8,128)(2,1)}), bf16[4,128,256]{1,2,0:T(8,128)(2,1)S(1)}, u32[]{:S(2)}, u32[]{:S(2)}) async-start(bf16[4,128,256]{1,2,0:T(8,128)(2,1)} %bitcast.11), calls=%async_computation | async-start | bytes 524288 | tf_op jit(solution)/shard_map/all_to_all | solution.py:86
  30.2 0.0 all-gather.5.cloned.1.call-start
  30.2 0.0 copy-done.2
  30.3 9.1 %all-to-all-done = bf16[4,128,256]{1,2,0:T(8,128)(2,1)S(1)} async-done(((bf16[4,128,256]{1,2,0:T(8,128)(2,1)}), bf16[4,128,256]{1,2,0:T(8,128)(2,1)S(1)}, u32[]{:S(2)}, u32[]{:S(2)}) %all-to-all-start) | async-done | bytes 262176 | tf_op jit(solution)/shard_map/all_to_all | solution.py:86
  39.4 9.6 %all-gather.3.cloned.1.call-done = bf16[1024,2048]{1,0:T(8,128)(2,1)} async-done(((bf16[256,2048]{1,0:T(8,128)(2,1)}), bf16[1024,2048]{1,0:T(8,128)(2,1)}) %all-gather.3.cloned.1.call-update) | async-done | bytes 4194320 | tf_op jit(solution)/shard_map/all_gather | solution.py:89
  48.9 0.0 copy-done
  48.9 3.0 %multiply_reduce_fusion = (f32[128]{0:T(128)S(1)}, f32[128,2048]{1,0:T(8,128)S(1)}) fusion(bf16[128,1024]{0,1:T(8,128)(2,1)S(1)} %bitcast.87, bf16[1024,2048]{1,0:T(8,128)(2,1)} %all-gather.3.cloned.1.call-done, bf16[128,2048]{1,0:T(8,128)(2,1)S(1)} %copy-done), kind=kOutput, calls=%fused_computation.18 | convolution fusion | flops 537919360 | bytes 6029824 | tf_op jit(solution)/shard_map/dot_general | solution.py:87
  51.9 0.0 copy-done.1
  52.0 0.6 convolution_convert_fusion.1
  52.5 37.2 %all_to_all.40 = bf16[8,40,2048]{2,1,0:T(8,128)(2,1)} all-to-all(bf16[8,40,2048]{2,1,0:T(8,128)(2,1)S(1)} %bitcast.85), channel_id=1, replica_groups=mesh['sp'=8,'tp'=4] {'sp'}, dimensions={0} | all-to-all | bytes 2621440 | tf_op jit(solution)/shard_map/all_to_all | solution.py:98
  89.7 0.0 all-gather.5.cloned.1.call-update
  89.7 0.0 reduce-scatter.2.cloned.1.call-start
  89.8 38.6 %all-gather.5.cloned.1.call-done = bf16[1280,2048]{1,0:T(8,128)(2,1)} async-done(((bf16[320,2048]{1,0:T(8,128)(2,1)}), bf16[1280,2048]{1,0:T(8,128)(2,1)}) %all-gather.5.cloned.1.call-update) | async-done | bytes 5242896 | tf_op jit(solution)/shard_map/all_gather | solution.py:99
  128.4 10.0 %fusion.2 = f32[1280,896]{1,0:T(8,128)} fusion(bf16[1280,2048]{1,0:T(8,128)(2,1)} %all-gather.5.cloned.1.call-done, bf16[1,2048,896]{2,1,0:T(8,128)(2,1)} %param.23), kind=kOutput, calls=%fused_computation.6 | convolution fusion | flops 4697620480 | bytes 13500416 | tf_op jit(solution)/shard_map/dot_general | solution.py:100
  138.4 17.6 %convolution_convert_fusion = bf16[1280,2048]{1,0:T(8,128)(2,1)} fusion(bf16[1,896,2048]{2,1,0:T(8,128)(2,1)} %param.25, f32[1280,896]{1,0:T(8,128)} %fusion.2, bf16[1280,2048]{1,0:T(8,128)(2,1)} %all-gather.5.cloned.1.call-done, bf16[1,2048,896]{2,1,0:T(8,128)(2,1)} %param.24), kind=kOutput, calls=%fused_computation.2 | convolution fusion | flops 9404743680 | bytes 22413312 | tf_op jit(solution)/shard_map/dot_general | solution.py:103
  155.9 0.0 copy-start.4
  155.9 0.0 reduce-scatter.2.cloned.1.call-update
  156.0 51.5 %reduce-scatter.2.cloned.1.call-done = bf16[320,2048]{1,0:T(8,128)(2,1)} async-done(((bf16[1280,2048]{1,0:T(8,128)(2,1)}), bf16[320,2048]{1,0:T(8,128)(2,1)}) %reduce-scatter.2.cloned.1.call-update) | async-done | bytes 1310736 | tf_op jit(solution)/shard_map/reduce_scatter | solution.py:104
  207.5 5.5 %all-to-all-start.2 = ((bf16[8,40,2048]{2,1,0:T(8,128)(2,1)}), bf16[8,40,2048]{2,1,0:T(8,128)(2,1)S(1)}, u32[]{:S(2)}, u32[]{:S(2)}) async-start(bf16[8,40,2048]{2,1,0:T(8,128)(2,1)} %bitcast.86), calls=%async_computation.3 | async-start | bytes 2621440 | tf_op jit(solution)/shard_map/all_to_all | solution.py:107
  213.0 0.0 copy-done.4
  213.0 31.2 %all-to-all-done.2 = bf16[8,40,2048]{2,1,0:T(8,128)(2,1)S(1)} async-done(((bf16[8,40,2048]{2,1,0:T(8,128)(2,1)}), bf16[8,40,2048]{2,1,0:T(8,128)(2,1)S(1)}, u32[]{:S(2)}, u32[]{:S(2)}) %all-to-all-start.2) | async-done | bytes 1310752 | tf_op jit(solution)/shard_map/all_to_all | solution.py:107
  244.2 0.9 gather_fusion
  245.1 0.9 gather_fusion.1
  246.1 1.2 add_convert_fusion
  (18 shorter events, 0.3 us)
Async XLA Ops:
  6.5 18.4 %copy-start.3 = (f32[4]{0:T(128)S(1)}, f32[4]{0:T(128)}, u32[]{:S(2)}) copy-start(f32[4]{0:T(128)} %param.17) | copy-start | bytes 52
  6.5 42.4 %all-gather.3.cloned.1.call-start = ((), (), s32[]{:S(2)}) async-start(), calls=%async_computation.4 | async-start | bytes 5242880 | tf_op jit(solution)/shard_map/all_gather | solution.py:89
  8.0 14.7 %collective-permute-start.1 = (bf16[128,64]{0,1:T(8,128)(2,1)S(1)}, bf16[128,64]{0,1:T(8,128)(2,1)S(1)}, u32[]{:S(2)}, u32[]{:S(2)}) collective-permute-start(bf16[128,64]{0,1:T(8,128)(2,1)S(1)} %slice.48), channel_id=1, source_target_pairs={{0,4},{4,8},{8,12},{12,16},{16,20},{20,24},{24,28},{1,5},{5,9},{9,... | collective-permute-start | bytes 49160 | tf_op jit(solution)/shard_map/ppermute | solution.py:16
  13.6 10.0 %collective-permute-start = (bf16[128,64]{0,1:T(8,128)(2,1)S(1)}, bf16[128,64]{0,1:T(8,128)(2,1)S(1)}, u32[]{:S(2)}, u32[]{:S(2)}) collective-permute-start(bf16[128,64]{0,1:T(8,128)(2,1)S(1)} %slice.44), channel_id=1, source_target_pairs={{0,4},{4,8},{8,12},{12,16},{16,20},{20,24},{24,28},{1,5},{5,9},{9,... | collective-permute-start | bytes 49160 | tf_op jit(solution)/shard_map/ppermute | solution.py:16
  25.4 4.8 %copy-start.2 = (s32[128,2]{0,1:T(2,128)S(1)}, s32[128,2]{0,1:T(2,128)}, u32[]{:S(2)}) copy-start(s32[128,2]{0,1:T(2,128)} %param.21) | copy-start | bytes 3076
  25.4 23.5 %copy-start = (bf16[128,2048]{1,0:T(8,128)(2,1)S(1)}, bf16[128,2048]{1,0:T(8,128)(2,1)}, u32[]{:S(2)}) copy-start(bf16[128,2048]{1,0:T(8,128)(2,1)} %param.18) | copy-start | bytes 1572868
  26.6 25.3 %copy-start.1 = (f32[2048]{0:T(1024)S(1)}, f32[2048]{0:T(1024)}, u32[]{:S(2)}) copy-start(f32[2048]{0:T(1024)} %param.20) | copy-start | bytes 24580
  26.6 12.7 %all-to-all-start = ((bf16[4,128,256]{1,2,0:T(8,128)(2,1)}), bf16[4,128,256]{1,2,0:T(8,128)(2,1)S(1)}, u32[]{:S(2)}, u32[]{:S(2)}) async-start(bf16[4,128,256]{1,2,0:T(8,128)(2,1)} %bitcast.11), calls=%async_computation | async-start | bytes 524288 | tf_op jit(solution)/shard_map/all_to_all | solution.py:86
  30.2 98.2 %all-gather.5.cloned.1.call-start = ((), (), s32[]{:S(2)}) async-start(), calls=%async_computation.5 | async-start | bytes 6553600 | tf_op jit(solution)/shard_map/all_gather | solution.py:99
  89.7 117.7 %reduce-scatter.2.cloned.1.call-start = ((), (), s32[]{:S(2)}) async-start(), calls=%async_computation.6 | async-start | bytes 6553600 | tf_op jit(solution)/shard_map/reduce_scatter | solution.py:104
  155.9 57.1 %copy-start.4 = (f32[128,2]{0,1:T(2,128)S(1)}, f32[128,2]{0,1:T(2,128)}, u32[]{:S(2)}) copy-start(f32[128,2]{0,1:T(2,128)} %param.22) | copy-start | bytes 3076
  207.5 36.7 %all-to-all-start.2 = ((bf16[8,40,2048]{2,1,0:T(8,128)(2,1)}), bf16[8,40,2048]{2,1,0:T(8,128)(2,1)S(1)}, u32[]{:S(2)}, u32[]{:S(2)}) async-start(bf16[8,40,2048]{2,1,0:T(8,128)(2,1)} %bitcast.86), calls=%async_computation.3 | async-start | bytes 2621440 | tf_op jit(solution)/shard_map/all_to_all | solution.py:107
Sparse Core Ops, SparseCore 0:
  8.9 39.9 all-gather.2
  89.8 38.5 all-gather.4
  156.1 51.3 reduce-scatter.1
where the time goes:
time: 255 us; the launch traced here: 254 us
  waiting for transfers between devices  141 us (55%)
  blocking collectives  37.2 us (15%)
  matrix products  32.9 us (13%)
  starting transfers between devices  17.4 us (7%)
  between operations  13.3 us (5%)
  local copies, waits for them, and re-layouts  7.91 us (3%)
  other arithmetic  4.42 us (2%)
    reduce_scatter x1, waiting for transfers between devices, on_device(): lax.psum_scatter(partial_value.astype(jnp.bfloat16), 'tp', scatter_dimens...  51.5 us
    all_gather x1, waiting for transfers between devices, on_device(): expert_input = lax.all_gather(arrived, 'tp', axis=0, tiled=True)  38.6 us
    all_to_all x1, blocking collectives, on_device(): lax.all_to_all(outgoing, 'sp', split_axis=0, concat_axis=0, tiled=True)  37.2 us
    all_to_all x1, waiting for transfers between devices, on_device(): lax.all_to_all(summed, 'sp', split_axis=0, concat_axis=0, tiled=True)  31.2 us
    dot_general x1, matrix products, on_device(): jnp.dot(hidden, down_proj[0], preferred_element_type=jnp.float32)  17.6 us
    dot_general x1, matrix products, on_device(): jnp.dot(expert_input, gate_proj[0], preferred_element_type=jnp.float32)  9.98 us
    all_gather x1, waiting for transfers between devices, on_device(): lax.all_gather(out_proj, 'tp', axis=0, tiled=True)  9.55 us
    all_to_all x1, waiting for transfers between devices, on_device(): lax.all_to_all(attended, 'tp', split_axis=0, concat_axis=1, tiled=True)  9.08 us
  transfers between devices with their start and end apart: 7, of which 5 were waited for; matrix products, arithmetic and copies ran while one was open for 4% of the time, Pallas kernels for 0%

commit v1 on v0

v1 whole, which is shorter than its diff:
```python
import functools

import jax
import jax.numpy as jnp
from jax import lax
from jax.experimental import pallas as pl
from jax.experimental.pallas import tpu as pltpu
from jax.sharding import PartitionSpec as P

DH = 64
WINDOW = 128
EPSILON = 1e-06
MESH = pl.DeviceIdType.MESH
F32 = jnp.float32
BF16 = jnp.bfloat16


def dot(a, b, dims=((1,), (0,))):
    return lax.dot_general(a, b, (dims, ((), ())), preferred_element_type=F32)


def greet(n, sp, partners):
    barrier = pltpu.get_barrier_semaphore()

    def hello(d, carry):
        pl.semaphore_signal(
            barrier, inc=1, device_id={"sp": lax.rem(sp + d, n)}, device_id_type=MESH
        )
        return carry

    lax.fori_loop(1, n, hello, 0)
    for t in partners:
        pl.semaphore_signal(barrier, inc=1, device_id={"tp": t}, device_id_type=MESH)
    pl.semaphore_wait(barrier, n - 1 + len(partners))


def slots_of(n, routes_t):
    rows = routes_t.shape[1]
    ids = lax.broadcasted_iota(jnp.int32, (n, rows), 0)
    hit = (routes_t[0:1, :] == ids) | (routes_t[1:2, :] == ids)
    before = lax.broadcasted_iota(jnp.int32, (rows, rows), 0) < lax.broadcasted_iota(
        jnp.int32, (rows, rows), 1
    )
    rank = dot(hit.astype(F32).astype(BF16), before.astype(F32).astype(BF16))
    return jnp.where(hit, rank, -1.0)


def picker_of(slot_row, cap):
    c = lax.broadcasted_iota(jnp.int32, (cap, slot_row.shape[1]), 0).astype(F32)
    return (slot_row == c).astype(F32).astype(BF16)


def front(
    n,
    q_ref,
    kv_ref,
    sink_ref,
    wo_ref,
    stream_ref,
    gain_ref,
    routes_ref,
    gate_ref,
    up_ref,
    down_ref,
    rows_ref,
    mixed_ref,
    gate_out,
    up_out,
    down_out,
    tail,
    wo_peer,
    att,
    att_peer,
    part_out,
    part_in,
    outgoing,
    normed,
    slots,
    one_send,
    one_recv,
    part_send,
    part_recv,
    out_send,
    out_recv,
    fwd_send,
    fwd_recv,
):
    sp = lax.axis_index("sp")
    tp = lax.axis_index("tp")
    lo = lax.rem(tp, 2)
    hi = tp // 2
    pair = 2 * hi + 1 - lo
    cross = 2 * (1 - hi) + lo
    tok = q_ref.shape[0]
    heads = q_ref.shape[1] // DH
    rows = stream_ref.shape[0]
    width = stream_ref.shape[1]
    cap = outgoing.shape[1]
    greet(n, sp, (pair, cross))

    def remote(src, dst, s, r, **where):
        return pltpu.make_async_remote_copy(
            src_ref=src, dst_ref=dst, send_sem=s, recv_sem=r, device_id=where, device_id_type=MESH
        )

    tail_copy = remote(
        kv_ref.at[pl.ds(tok - WINDOW, WINDOW)],
        tail,
        one_send.at[0],
        one_recv.at[0],
        sp=lax.rem(sp + 1, n),
    )
    tail_copy.start()
    wo_copy = remote(wo_ref, wo_peer, one_send.at[1], one_recv.at[1], tp=pair)
    wo_copy.start()

    slots[...] = slots_of(n, routes_ref[...])
    query = lax.broadcasted_iota(jnp.int32, (WINDOW, 2 * WINDOW), 0) + WINDOW
    key = lax.broadcasted_iota(jnp.int32, (WINDOW, 2 * WINDOW), 1)
    inside = (query - key >= 0) & (query - key < WINDOW)
    blocks = tok // WINDOW
    for b in list(range(1, blocks)) + [0]:
        if b == 0:
            tail_copy.wait()
            band = jnp.concatenate([tail[...], kv_ref[pl.ds(0, WINDOW), :]], axis=0)
            allowed = inside & ((key >= WINDOW) | (sp > 0))
        else:
            band = kv_ref[pl.ds((b - 1) * WINDOW, 2 * WINDOW), :]
            allowed = inside
        pieces = []
        kb, vb = band[:, :DH], band[:, DH:]
        qb = q_ref[pl.ds(b * WINDOW, WINDOW), :]
        for h in range(heads):
            score = dot(qb[:, h * DH : (h + 1) * DH], kb, ((1,), (1,))) * DH ** (-0.5)
            score = jnp.where(allowed, score, -jnp.inf)
            sink = sink_ref[h]
            top = jnp.maximum(jnp.max(score, axis=-1, keepdims=True), sink)
            expo = jnp.exp(score - top)
            denom = jnp.sum(expo, axis=-1, keepdims=True) + jnp.exp(sink - top)
            pieces.append(dot((expo / denom).astype(BF16), vb))
        att[pl.ds(b * WINDOW, WINDOW), :] = jnp.concatenate(pieces, axis=1).astype(BF16)

    att_copies = []
    for g in range(2):
        where = pl.multiple_of((2 * g + 1 - lo) * rows, rows)
        copy = remote(
            att.at[pl.ds(where, rows)],
            att_peer.at[g],
            one_send.at[2 + g],
            one_recv.at[2 + g],
            tp=pair,
        )
        copy.start()
        att_copies.append(copy)
    weight_copies = []
    for k, (src, dst) in enumerate(((gate_ref, gate_out), (up_ref, up_out), (down_ref, down_out))):
        copy = remote(src, dst, one_send.at[4 + k], one_recv.at[4 + k], tp=pair)
        copy.start()
        weight_copies.append(copy)
    wo_copy.wait()
    for copy in att_copies:
        copy.wait()

    chunk = width // 4
    part_copies = []
    mine = att[pl.ds(pl.multiple_of(cross * rows, rows), rows), :]
    theirs = att_peer[1 - hi]
    for k in range(4):
        cols = pl.ds(k * chunk, chunk)
        part_out[k] = (dot(mine, wo_ref[:, cols]) + dot(theirs, wo_peer[:, cols])).astype(BF16)
        copy = remote(part_out.at[k], part_in.at[k], part_send.at[k], part_recv.at[k], tp=cross)
        copy.start()
        part_copies.append(copy)
    mine = att[pl.ds(pl.multiple_of(tp * rows, rows), rows), :]
    theirs = att_peer[hi]
    for k in range(4):
        cols = pl.ds(k * chunk, chunk)
        mixed_ref[:, cols] = (
            stream_ref[:, cols].astype(F32)
            + dot(mine, wo_ref[:, cols])
            + dot(theirs, wo_peer[:, cols])
        )
    square = jnp.zeros((rows, 1), F32)
    for k in range(4):
        cols = pl.ds(k * chunk, chunk)
        part_copies[k].wait()
        value = mixed_ref[:, cols] + part_in[k].astype(F32)
        mixed_ref[:, cols] = value
        square = square + jnp.sum(value * value, axis=-1, keepdims=True)
    scale = lax.rsqrt(square / width + EPSILON)
    for k in range(4):
        cols = pl.ds(k * chunk, chunk)
        normed[:, cols] = (mixed_ref[:, cols] * scale * gain_ref[:, cols]).astype(BF16)

    def sent(d):
        e = lax.rem(sp + d, n)
        return remote(outgoing.at[e], rows_ref.at[0, sp], out_send.at[d], out_recv.at[d], sp=e)

    def arrival(d):
        s = lax.rem(sp + n - d, n)
        return remote(outgoing.at[s], rows_ref.at[0, s], out_send.at[d], out_recv.at[d], sp=s)

    def forward(d):
        s = lax.rem(sp + n - d, n)
        return remote(
            rows_ref.at[0, s], rows_ref.at[1, s], fwd_send.at[d], fwd_recv.at[d], tp=cross
        )

    def pick(e):
        picker = picker_of(slots[pl.ds(e, 1), :], cap)
        return dot(picker, normed[...]).astype(BF16)

    rows_ref[0, sp] = pick(sp)
    forward(0).start()

    def send(i, carry):
        e = lax.rem(sp + i, n)
        outgoing[e] = pick(e)
        sent(i).start()
        return carry

    lax.fori_loop(1, n, send, 0)

    def relay(d, carry):
        arrival(d).wait_recv()
        forward(d).start()
        return carry

    lax.fori_loop(1, n, relay, 0)

    def finish(d, carry):
        sent(d).wait_send()
        return carry

    lax.fori_loop(1, n, finish, 0)

    def finish_forward(d, carry):
        forward(d).wait()
        return carry

    lax.fori_loop(0, n, finish_forward, 0)
    for copy in weight_copies:
        copy.wait()


def back(
    n,
    partial_ref,
    mixed_ref,
    routes_ref,
    routes_t_ref,
    weights_ref,
    out_ref,
    peer,
    outgoing,
    returned,
    total,
    slots,
    pair_send,
    pair_recv,
    out_send,
    out_recv,
):
    sp = lax.axis_index("sp")
    tp = lax.axis_index("tp")
    lo = lax.rem(tp, 2)
    cross = 2 * (1 - tp // 2) + lo
    cap = outgoing.shape[1]
    greet(n, sp, (cross,))

    def remote(src, dst, s, r, **where):
        return pltpu.make_async_remote_copy(
            src_ref=src, dst_ref=dst, send_sem=s, recv_sem=r, device_id=where, device_id_type=MESH
        )

    def swap(d):
        s = lax.rem(sp + d, n)
        return remote(partial_ref.at[1, s], peer.at[s], pair_send.at[d], pair_recv.at[d], tp=cross)

    def sent(d):
        s = lax.rem(sp + d, n)
        return remote(outgoing.at[s], returned.at[sp], out_send.at[d], out_recv.at[d], sp=s)

    def arrival(d):
        e = lax.rem(sp + n - d, n)
        return remote(outgoing.at[e], returned.at[e], out_send.at[d], out_recv.at[d], sp=e)

    def begin(i, carry):
        swap(lax.rem(i, n)).start()
        return carry

    lax.fori_loop(1, n + 1, begin, 0)
    slots[...] = slots_of(n, routes_t_ref[...])
    total[...] = mixed_ref[...]

    def summed(s):
        return (partial_ref[0, s].astype(F32) + peer[s].astype(F32)).astype(BF16)

    def send(d, carry):
        swap(d).wait()
        s = lax.rem(sp + d, n)
        outgoing[s] = summed(s)
        sent(d).start()
        return carry

    lax.fori_loop(1, n, send, 0)
    swap(0).wait()
    returned[sp] = summed(sp)
    routes = routes_ref[...]
    weights = weights_ref[...]

    def add(e):
        picker = picker_of(slots[pl.ds(e, 1), :], cap)
        weight = jnp.sum(jnp.where(routes == e, weights, 0.0), axis=1, keepdims=True)
        total[...] += weight * dot(picker, returned[e], ((0,), (0,)))

    add(sp)

    def gather(d, carry):
        arrival(d).wait_recv()
        add(lax.rem(sp + n - d, n))
        return carry

    lax.fori_loop(1, n, gather, 0)

    def finish(d, carry):
        sent(d).wait_send()
        return carry

    lax.fori_loop(1, n, finish, 0)
    out_ref[...] = total[...].astype(BF16)


def on_device(
    queries,
    keys,
    values,
    sink_logits,
    stream,
    out_proj,
    norm_gain,
    routes,
    route_weights,
    gate_proj,
    up_proj,
    down_proj,
):
    n = lax.axis_size("sp")
    tok_sp, att_width = queries.shape
    rows, width = stream.shape
    capacity = max(2, (5 * rows + 2 * n - 1) // (2 * n))
    cap = -(-capacity // 8) * 8
    kv = jnp.concatenate([keys, values], axis=1)
    routes_t = routes.T
    gate, up, down = gate_proj[0], up_proj[0], down_proj[0]
    vmem = pl.BlockSpec(memory_space=pltpu.VMEM)
    smem = pl.BlockSpec(memory_space=pltpu.SMEM)
    anywhere = pl.BlockSpec(memory_space=pltpu.HBM)
    dma = pltpu.SemaphoreType.DMA
    like = jax.ShapeDtypeStruct
    arrived, mixed, gate_two, up_two, down_two = pl.pallas_call(
        functools.partial(front, n),
        out_shape=(
            like((2, n, cap, width), BF16),
            like((rows, width), F32),
            like(gate.shape, BF16),
            like(up.shape, BF16),
            like(down.shape, BF16),
        ),
        in_specs=[vmem, vmem, smem, vmem, vmem, vmem, vmem, anywhere, anywhere, anywhere],
        out_specs=(vmem, vmem, anywhere, anywhere, anywhere),
        scratch_shapes=[
            pltpu.VMEM((WINDOW, 2 * DH), BF16),
            pltpu.VMEM(out_proj.shape, BF16),
            pltpu.VMEM((tok_sp, att_width), BF16),
            pltpu.VMEM((2, rows, att_width), BF16),
            pltpu.VMEM((4, rows, width // 4), BF16),
            pltpu.VMEM((4, rows, width // 4), BF16),
            pltpu.VMEM((n, cap, width), BF16),
            pltpu.VMEM((rows, width), BF16),
            pltpu.VMEM((n, rows), F32),
            dma((7,)),
            dma((7,)),
            dma((4,)),
            dma((4,)),
            dma((n,)),
            dma((n,)),
            dma((n,)),
            dma((n,)),
        ],
        compiler_params=pltpu.CompilerParams(collective_id=0, has_side_effects=True),
        name="front",
    )(
        queries,
        kv,
        sink_logits,
        out_proj,
        stream,
        norm_gain.reshape(1, width),
        routes_t,
        gate,
        up,
        down,
    )
    expert_rows = arrived.reshape(2 * n * cap, width)

    def expert(g, u):
        gate_part = jnp.dot(expert_rows, g, preferred_element_type=F32)
        up_part = jnp.dot(expert_rows, u, preferred_element_type=F32)
        return (jax.nn.silu(gate_part) * up_part).astype(BF16)

    partial_value = jnp.dot(expert(gate, up), down, preferred_element_type=F32) + jnp.dot(
        expert(gate_two, up_two), down_two, preferred_element_type=F32
    )
    partial_value = partial_value.astype(BF16).reshape(2, n, cap, width)
    return pl.pallas_call(
        functools.partial(back, n),
        out_shape=like((rows, width), BF16),
        in_specs=[vmem] * 5,
        out_specs=vmem,
        scratch_shapes=[
            pltpu.VMEM((n, cap, width), BF16),
            pltpu.VMEM((n, cap, width), BF16),
            pltpu.VMEM((n, cap, width), BF16),
            pltpu.VMEM((rows, width), F32),
            pltpu.VMEM((n, rows), F32),
            dma((n,)),
            dma((n,)),
            dma((n,)),
            dma((n,)),
        ],
        compiler_params=pltpu.CompilerParams(collective_id=1, has_side_effects=True),
        name="back",
    )(partial_value, mixed, routes, routes_t, route_weights)


def solution(mesh):
    return jax.shard_map(
        on_device,
        mesh=mesh,
        in_specs=(
            P("sp", "tp"),
            P("sp", "tp"),
            P("sp", "tp"),
            P("tp"),
            P(("sp", "tp"), None),
            P("tp", None),
            P(),
            P(("sp", "tp"), None),
            P(("sp", "tp"), None),
            P("sp", None, "tp"),
            P("sp", None, "tp"),
            P("sp", "tp", None),
        ),
        out_specs=P(("sp", "tp"), None),
        check_vma=False,
    )
```

time: 255 us -> 158 us (0.62)
  waiting for transfers between devices: 141 us -> 0 us
  Pallas kernels: 0 us -> 113 us
  blocking collectives: 37.2 us -> 0 us
  starting transfers between devices: 17.4 us -> 0 us
  between operations: 13.3 us -> 0.05 us
  other arithmetic: 4.42 us -> 0.77 us
  matrix products: 32.9 us -> 35.7 us
    pallas_call x0 -> x2, Pallas kernels: none -> 113 us  [the longest x1 67.7 us: on_device(): pl.pallas_call(functools.partial(front, n), out_shape=(like((2, n, cap, w...]
    reduce_scatter x1 -> x0, waiting for transfers between devices: 51.5 us -> none  [on_device(): lax.psum_scatter(partial_value.astype(jnp.bfloat16), 'tp', scatter_dimens...]
    all_gather x2 -> x0, waiting for transfers between devices: 48.2 us -> none  [the longest x1 38.6 us: on_device(): expert_input = lax.all_gather(arrived, 'tp', axis=0, tiled=True)]
    all_to_all x2 -> x0, waiting for transfers between devices: 40.3 us -> none  [the longest x1 31.2 us: on_device(): lax.all_to_all(summed, 'sp', split_axis=0, concat_axis=0, tiled=True)]
    all_to_all x1 -> x0, blocking collectives: 37.2 us -> none  [on_device(): lax.all_to_all(outgoing, 'sp', split_axis=0, concat_axis=0, tiled=True)]
    all_to_all x2 -> x0, starting transfers between devices: 9.05 us -> none  [the longest x1 5.51 us: on_device(): lax.all_to_all(summed, 'sp', split_axis=0, concat_axis=0, tiled=True)]
    ppermute x2 -> x0, starting transfers between devices: 8.3 us -> none  [from_behind(): return lax.ppermute(value, axis, pairs)]
    unnamed x11 -> x9, local copies, waits for them, and re-layouts: 0.81 us -> 6.63 us
  transfers between devices with their start and end apart: 7 -> 0, of which waited for: 5 -> 0; matrix products, arithmetic and copies ran while one was open for 4% -> 0% of each run, Pallas kernels for 0% -> 0%
where the time goes in v1:
time: 158 us; the launch traced here: 156 us
  Pallas kernels  113 us (72%)
  matrix products  35.7 us (23%)
  local copies, waits for them, and re-layouts  6.63 us (4%)
    pallas_call x1, Pallas kernels, on_device(): pl.pallas_call(functools.partial(front, n), out_shape=(like((2, n, cap, w...  67.7 us
    pallas_call x1, Pallas kernels, on_device(): pl.pallas_call(functools.partial(back, n), out_shape=like((rows, width),...  45 us
    dot_general x1, matrix products, on_device(): jnp.dot(expert(gate_two, up_two), down_two, preferred_element_type=F32)  12.4 us
    dot_general x1, matrix products, on_device(): jnp.dot(expert(gate, up), down, preferred_element_type=F32)  11.8 us
    dot_general x2, matrix products, expert(): gate_part = jnp.dot(expert_rows, g, preferred_element_type=F32)  11.5 us
    unnamed x9, local copies, waits for them, and re-layouts  6.63 us

profile of v1, /device:TPU:0, one launch (start us, length us, event | category | flops | bytes accessed | tf_op | source)
XLA Modules:
  0.0 155.8 jit_solution(15375374618582738933)
XLA Ops:
  0.0 1.4 copy.16.weights_ref
  1.4 1.4 copy.15.routes_ref
  2.8 1.0 copy.13
  3.8 1.0 copy.14
  4.7 0.8 pad_maximum_fusion.kv_ref
  5.5 67.7 %front.1 = (bf16[2,8,40,2048]{3,2,1,0:T(8,128)(2,1)}, f32[128,2048]{1,0:T(8,128)}, bf16[2048,896]{1,0:T(8,128)(2,1)}, bf16[2048,896]{1,0:T(8,128)(2,1)}, bf16[896,2048]{1,0:T(8,128)(2,1)}) custom-call(bf16[512,256]{1,0:T(8,128)(2,1)} %q_ref.1, bf16[512,128]{1,0:T(8,128)(2,1)} %pad_maximum_fusion.kv_ref, f32[4]{0:T(128)} %sink_ref.1, ...), custom_call_target="tpu_custom_call" | custom-call | tf_op jit(solution)/shard_map/front/pallas_call | solution.py:361
  73.3 0.0 copy-start
  73.3 0.0 copy-start.1
  73.3 7.2 %fusion.8 = f32[640,896]{1,0:T(8,128)} fusion(bf16[640,2048]{1,0:T(8,128)(2,1)} %bitcast.28, bf16[2048,896]{1,0:T(8,128)(2,1)} %get-tuple-element.11), kind=kOutput, calls=%fused_computation.11 | convolution fusion | flops 2348810240 | bytes 8585216 | tf_op jit(solution)/shard_map/dot_general | solution.py:408
  80.5 0.0 copy-done
  80.5 0.0 copy-done.1
  80.5 4.3 %fusion.4 = f32[640,896]{1,0:T(8,128)} fusion(bf16[640,2048]{1,0:T(8,128)(2,1)S(1)} %bitcast.29, bf16[1,2048,896]{2,1,0:T(8,128)(2,1)S(1)} %copy-done), kind=kOutput, calls=%fused_computation.7 | convolution fusion | flops 2348810240 | bytes 8585216 | tf_op jit(solution)/shard_map/dot_general | solution.py:408
  84.8 11.8 %fusion = f32[640,2048]{1,0:T(8,128)} fusion(f32[640,896]{1,0:T(8,128)} %fusion.4, bf16[640,2048]{1,0:T(8,128)(2,1)S(1)} %bitcast.30, bf16[1,896,2048]{2,1,0:T(8,128)(2,1)} %param.23, bf16[1,2048,896]{2,1,0:T(8,128)(2,1)} %param.22), kind=kOutput, calls=%fused_computation.3 | convolution fusion | flops 4701061120 | bytes 17498112 | tf_op jit(solution)/shard_map/dot_general | solution.py:412
  96.5 12.4 %add_convert_fusion = bf16[640,2048]{1,0:T(8,128)(2,1)} fusion(f32[640,2048]{1,0:T(8,128)} %fusion, bf16[896,2048]{1,0:T(8,128)(2,1)} %get-tuple-element.13, f32[640,896]{1,0:T(8,128)} %fusion.8, bf16[640,2048]{1,0:T(8,128)(2,1)S(1)} %bitcast.31, bf16[2048,896]{1,0:T(8,128)(2,1)} %get-tuple-element.12), kind=kOutput, calls=%fused_computation | convolution fusion | flops 4703682560 | bytes 20119552 | tf_op jit(solution)/shard_map/dot_general | solution.py:412
  109.0 45.0 %back.1 = bf16[128,2048]{1,0:T(8,128)(2,1)} custom-call(bf16[2,8,40,2048]{3,2,1,0:T(8,128)(2,1)} %bitcast.24, f32[128,2048]{1,0:T(8,128)} %get-tuple-element.14.mixed_ref, s32[128,2]{1,0:T(8,128)} %copy.15.routes_ref, s32[2,128]{1,0:T(2,128)} %bitcast.26, f32[128,2]{1,0:T(8,128)} %copy.16.weights_ref), custom_call_target="tpu_custom_call" | custom-call | tf_op jit(solution)/shard_map/back/pallas_call | solution.py:416
  154.0 1.9 %copy.18 = bf16[128,2048]{1,0:T(8,128)(2,1)} copy(bf16[128,2048]{1,0:T(8,128)(2,1)} %back.1) | data formatting | bytes 1048576
Async XLA Ops:
  73.3 7.2 %copy-start = (bf16[1,2048,896]{2,1,0:T(8,128)(2,1)S(1)}, bf16[1,2048,896]{2,1,0:T(8,128)(2,1)}, u32[]{:S(2)}) copy-start(bf16[1,2048,896]{2,1,0:T(8,128)(2,1)} %param.21) | copy-start | bytes 11010052
  73.3 7.2 %copy-start.1 = (bf16[2,8,40,2048]{3,2,1,0:T(8,128)(2,1)S(1)}, bf16[2,8,40,2048]{3,2,1,0:T(8,128)(2,1)}, u32[]{:S(2)}) copy-start(bf16[2,8,40,2048]{3,2,1,0:T(8,128)(2,1)} %get-tuple-element.10) | copy-start | bytes 7864324
